TPU v7x, 32 devices: a whole 2x2x4 slice. The times are simulated.
32 devices in a mesh: ep: 8 (over z, core), tp: 4 (over y, x).
Axes of the slice: x: 2, y: 2, z: 4, core: 2. Of those that a mesh axis runs over, the one named last changes fastest.
Arguments:
- tokens: bfloat16 [2048, 2048], P('ep'), may hold values from -6 to 6
- norm_gain: float32 [2048], replicated, may hold values from 0.1 to 1.9
- route_ids: int32 [2048, 4], P('ep'), may hold values from 0 to 15, all different within a row; in each aligned block of 256 rows (0 to 255, 256 to 511, ...) at most 96 rows name the same one
- route_weights: float32 [2048, 4], P('ep'), may hold values from 0.1 to 1
- w_gate: bfloat16 [16, 2048, 2048], P('ep', None, 'tp'), may hold values from -0.33007812 to 0.33007812
- w_up: bfloat16 [16, 2048, 2048], P('ep', None, 'tp'), may hold values from -0.33007812 to 0.33007812
- w_down: bfloat16 [16, 2048, 2048], P('ep', None, 'tp'), may hold values from -0.026489258 to 0.026489258
Outputs:
- mixed_out: bfloat16 [2048, 2048], P('ep', 'tp')
Inputs may be any that keep to these rules, and one draw needn't show every extreme that they name: `route_ids`: each token names 4 different experts. Within the tokens of one index of ep (aligned blocks of 256 tokens) no expert is named more than 96 times, a bound that some block reaches.
All inputs are finite; a program needn't handle non-finite values.
Results may differ from a plain program's by a relative error of at most 0.007.
Values may be sent and summed in bfloat16 or wider, within the bound.
A program may use at most 64 MiB of HBM per device.

v0:
```python
import jax
import jax.numpy as jnp
from jax import lax
from jax.sharding import PartitionSpec as P

swiglu_limit = 7.0
swiglu_alpha = 1.702
norm_eps = 1e-05


def clamped_units(gate_pre, up_pre):
    capped = jnp.minimum(gate_pre, swiglu_limit)
    linear = jnp.clip(up_pre, -swiglu_limit, swiglu_limit)
    return capped * jax.nn.sigmoid(swiglu_alpha * capped) * (linear + 1.0)


def expert_work(outgoing, gate_weight, up_weight, down_weight):
    received = lax.all_to_all(outgoing, "ep", split_axis=1, concat_axis=1, tiled=True)
    local_count, sources, capacity, columns = received.shape
    row_count = sources * capacity
    row_block = received.reshape(local_count, row_count, columns)
    shard_piece = lax.all_gather(row_block, "tp", axis=2, tiled=True)
    gate_sum = jnp.einsum(
        "lrd,ldf->lrf", shard_piece, gate_weight, preferred_element_type=jnp.float32
    )
    up_sum = jnp.einsum("lrd,ldf->lrf", shard_piece, up_weight, preferred_element_type=jnp.float32)
    activation = clamped_units(gate_sum, up_sum).astype(jnp.bfloat16)
    out_cols = down_weight.shape[2]
    result = jnp.einsum(
        "lrf,lfd->lrd",
        lax.all_gather(activation, "tp", axis=2, tiled=True),
        down_weight,
        preferred_element_type=jnp.float32,
    )
    result = result.astype(jnp.bfloat16).reshape(local_count, sources, capacity, out_cols)
    return lax.all_to_all(result, "ep", split_axis=1, concat_axis=1, tiled=True)


def per_device(tokens, norm_gain, route_ids, route_weights, w_gate, w_up, w_down):
    local_count = w_gate.shape[0]
    sources = lax.axis_size("ep")
    tp_count = lax.axis_size("tp")
    width = tokens.shape[1]
    columns = width // tp_count
    experts = local_count * sources
    tok_rows, top_count = route_ids.shape
    capacity = 3 * tok_rows * top_count // (2 * experts)
    values = tokens.astype(jnp.float32)
    row_mean = jnp.mean(values, axis=1, keepdims=True)
    centred = values - row_mean
    row_var = jnp.mean(centred * centred, axis=1, keepdims=True)
    offset = lax.axis_index("tp") * columns
    own_cols = lax.dynamic_slice_in_dim(centred, offset, columns, 1)
    own_gain = lax.dynamic_slice_in_dim(norm_gain, offset, columns, 0)
    normed = (own_cols * lax.rsqrt(row_var + norm_eps) * own_gain).astype(jnp.bfloat16)
    flat_ids = route_ids.reshape(-1)
    matches = (flat_ids[:, None] == jnp.arange(experts, dtype=jnp.int32)[None, :]).astype(jnp.int32)
    earlier = jnp.cumsum(matches, axis=0) - matches
    slot_index = jnp.sum(earlier * matches, axis=1)
    position = (
        flat_ids % local_count * (sources * capacity)
        + flat_ids // local_count * capacity
        + slot_index
    )
    buffer_rows = local_count * sources * capacity
    placed = (
        position.reshape(tok_rows, top_count)[:, :, None]
        == jnp.arange(buffer_rows, dtype=jnp.int32)[None, None, :]
    )
    placement_matrix = jnp.any(placed, axis=1).astype(jnp.bfloat16)
    outgoing = jnp.einsum("tp,td->pd", placement_matrix, normed, preferred_element_type=jnp.float32)
    outgoing = outgoing.astype(jnp.bfloat16).reshape(local_count, sources, capacity, columns)
    returned = jnp.concatenate(
        [
            expert_work(
                outgoing[number : number + 1],
                w_gate[number : number + 1],
                w_up[number : number + 1],
                w_down[number : number + 1],
            )
            for number in range(local_count)
        ],
        axis=0,
    )
    flat_out = returned.reshape(buffer_rows, columns)
    picked = flat_out[position].reshape(tok_rows, top_count, columns).astype(jnp.float32)
    return jnp.sum(picked * route_weights[:, :, None], axis=1).astype(jnp.bfloat16)


def solution(mesh):
    return jax.shard_map(
        per_device,
        mesh=mesh,
        in_specs=(
            P("ep", None),
            P(),
            P("ep", None),
            P("ep", None),
            P("ep", None, "tp"),
            P("ep", None, "tp"),
            P("ep", None, "tp"),
        ),
        out_specs=P("ep", "tp"),
        check_vma=False,
    )
```

profile of v0, /device:TPU:0, one launch (start us, length us, event | category | flops | bytes accessed | tf_op | source)
XLA Modules:
  0.0 269.5 jit_solution(14024327743090888040)
XLA Ops:
  6.5 0.0 copy-start
  6.5 0.0 all-gather.7.cloned.1.call-start
  6.5 0.9 copy.62
  7.4 0.1 eq.44
  7.6 0.1 eq.40
  7.7 4.5 %reduce-window.6 = s32[16,8,128]{2,1,0:T(8,128)S(1)} reduce-window(s32[16,8,128]{2,1,0:T(8,128)S(1)} %fusion.42, s32[]{:T(128)} %constant.28.clone.1), window={size=1x1x128 pad=0_0x0_0x127_0}, to_apply=%region_0.0 | reduce-window | flops 2080768 | bytes 131076 | tf_op jit(solution)/shard_map/reduce-window
  12.2 0.1 slice.50
  12.3 0.1 copy.64
  12.5 0.1 copy.65
  12.5 0.1 broadcast_add_fusion
  12.7 0.1 reduce_sum.41
  12.8 0.1 copy.66
  12.9 0.7 fusion.45
  13.6 1.7 fusion
  15.3 0.0 copy-done
  15.3 0.2 convert_reduce_fusion
  15.6 0.4 multiply_reduce_fusion.1
  16.0 0.8 dynamic_slice.7
  16.8 1.7 convolution_convert_fusion
  18.5 0.1 fusion.53
  18.6 27.2 %all_to_all.20 = bf16[1,8,96,512]{3,2,0,1:T(8,128)(2,1)} all-to-all(bf16[1,8,96,512]{3,2,0,1:T(8,128)(2,1)S(1)} %bitcast.82), channel_id=1, replica_groups=mesh['ep'=8,'tp'=4] {'ep'}, dimensions={1} | all-to-all | bytes 1572864 | tf_op jit(solution)/shard_map/all_to_all | solution.py:18
  45.8 0.0 all-gather.7.cloned.1.call-update
  45.8 0.0 all-gather.9.cloned.1.call-start
  45.9 24.0 %all_to_all.21 = bf16[1,8,96,512]{3,2,0,1:T(8,128)(2,1)} all-to-all(bf16[1,8,96,512]{3,2,0,1:T(8,128)(2,1)S(1)} %bitcast.81), channel_id=1, replica_groups=mesh['ep'=8,'tp'=4] {'ep'}, dimensions={1} | all-to-all | bytes 1572864 | tf_op jit(solution)/shard_map/all_to_all | solution.py:18
  69.9 0.0 all-gather.9.cloned.1.call-update
  69.9 0.0 all-gather.11.cloned.1.call-start
  70.0 18.6 %all-gather.7.cloned.1.call-done = bf16[1,768,2048]{2,1,0:T(8,128)(2,1)} async-done(((bf16[1,768,512]{2,1,0:T(8,128)(2,1)}), bf16[1,768,2048]{2,1,0:T(8,128)(2,1)}) %all-gather.7.cloned.1.call-update) | async-done | bytes 3145744 | tf_op jit(solution)/shard_map/all_gather | solution.py:22
  88.6 0.0 copy-start.2
  88.6 0.0 copy-start.5
  88.6 4.5 %fusion.7 = f32[768,512]{1,0:T(8,128)S(1)} fusion(bf16[1,768,2048]{2,1,0:T(8,128)(2,1)} %all-gather.7.cloned.1.call-done, bf16[2,2048,512]{2,1,0:T(8,128)(2,1)} %param.11), kind=kOutput, calls=%fused_computation.9 | convolution fusion | flops 1610612736 | bytes 6815744 | tf_op jit(solution)/shard_map/lrd,ldf->lrf/dot_general | solution.py:23
  93.1 0.0 copy-done.2
  93.1 0.2 copy-done.5
  93.3 3.0 %multiply_convert_fusion.1 = bf16[768,512]{1,0:T(8,128)(2,1)} fusion(f32[768,512]{1,0:T(8,128)S(1)} %fusion.7, bf16[2,2048,512]{2,1,0:T(8,128)(2,1)S(1)} %copy-done.2, bf16[1,768,2048]{2,1,0:T(8,128)(2,1)S(1)} %copy-done.5), kind=kOutput, calls=%fused_computation.32 | convolution fusion | flops 1614544896 | bytes 7602176 | tf_op jit(solution)/shard_map/lrd,ldf->lrf/dot_general | solution.py:26
  96.3 0.0 all-gather.11.cloned.1.call-update
  96.4 0.0 all-gather.13.cloned.1.call-start
  96.4 37.8 %all-gather.9.cloned.1.call-done = bf16[1,768,2048]{2,1,0:T(8,128)(2,1)} async-done(((bf16[1,768,512]{2,1,0:T(8,128)(2,1)}), bf16[1,768,2048]{2,1,0:T(8,128)(2,1)}) %all-gather.9.cloned.1.call-update) | async-done | bytes 3145744 | tf_op jit(solution)/shard_map/all_gather | solution.py:22
  134.2 0.0 copy-start.3
  134.2 0.0 copy-start.4
  134.2 4.5 %fusion.3 = f32[768,512]{1,0:T(8,128)S(1)} fusion(bf16[1,768,2048]{2,1,0:T(8,128)(2,1)} %all-gather.9.cloned.1.call-done, bf16[2,2048,512]{2,1,0:T(8,128)(2,1)} %param.11), kind=kOutput, calls=%fused_computation.5 | convolution fusion | flops 1610612736 | bytes 6815744 | tf_op jit(solution)/shard_map/lrd,ldf->lrf/dot_general | solution.py:23
  138.7 0.0 copy-done.3
  138.7 0.2 copy-done.4
  138.9 3.0 %multiply_convert_fusion = bf16[768,512]{1,0:T(8,128)(2,1)} fusion(f32[768,512]{1,0:T(8,128)S(1)} %fusion.3, bf16[2,2048,512]{2,1,0:T(8,128)(2,1)S(1)} %copy-done.3, bf16[1,768,2048]{2,1,0:T(8,128)(2,1)S(1)} %copy-done.4), kind=kOutput, calls=%fused_computation.31 | convolution fusion | flops 1614544896 | bytes 7602176 | tf_op jit(solution)/shard_map/lrd,ldf->lrf/dot_general | solution.py:26
  141.9 0.0 all-gather.13.cloned.1.call-update
  141.9 37.8 %all-gather.11.cloned.1.call-done = bf16[768,2048]{1,0:T(8,128)(2,1)} async-done(((bf16[768,512]{1,0:T(8,128)(2,1)}), bf16[768,2048]{1,0:T(8,128)(2,1)}) %all-gather.11.cloned.1.call-update) | async-done | bytes 3145744 | tf_op jit(solution)/shard_map/all_gather | solution.py:31
  179.8 5.2 %fusion.31 = bf16[768,512]{1,0:T(8,128)(2,1)} fusion(bf16[768,2048]{1,0:T(8,128)(2,1)} %all-gather.11.cloned.1.call-done, bf16[2,2048,512]{2,1,0:T(8,128)(2,1)} %param.13), kind=kOutput, calls=%fused_computation.33 | convolution fusion | flops 1611005952 | bytes 6029312 | tf_op jit(solution)/shard_map/lrf,lfd->lrd/dot_general | solution.py:29
  185.0 4.6 %all-to-all-start.1 = ((bf16[1,8,96,512]{3,2,0,1:T(8,128)(2,1)}), bf16[1,8,96,512]{3,2,0,1:T(8,128)(2,1)S(1)}, u32[]{:S(2)}, u32[]{:S(2)}) async-start(bf16[1,8,96,512]{3,2,0,1:T(8,128)(2,1)} %bitcast.10), calls=%async_computation.1 | async-start | bytes 1572864 | tf_op jit(solution)/shard_map/all_to_all | solution.py:36
  189.6 0.0 copy-start.1
  189.6 35.6 %all-gather.13.cloned.1.call-done = bf16[768,2048]{1,0:T(8,128)(2,1)} async-done(((bf16[768,512]{1,0:T(8,128)(2,1)}), bf16[768,2048]{1,0:T(8,128)(2,1)}) %all-gather.13.cloned.1.call-update) | async-done | bytes 3145744 | tf_op jit(solution)/shard_map/all_gather | solution.py:31
  225.2 5.2 %fusion.34 = bf16[768,512]{1,0:T(8,128)(2,1)} fusion(bf16[768,2048]{1,0:T(8,128)(2,1)} %all-gather.13.cloned.1.call-done, bf16[2,2048,512]{2,1,0:T(8,128)(2,1)} %param.13), kind=kOutput, calls=%fused_computation.34 | convolution fusion | flops 1611005952 | bytes 6029312 | tf_op jit(solution)/shard_map/lrf,lfd->lrd/dot_general | solution.py:29
  230.4 0.0 all-to-all-done.1
  230.4 4.6 %all-to-all-start.3 = ((bf16[1,8,96,512]{3,2,0,1:T(8,128)(2,1)}), bf16[1,8,96,512]{3,2,0,1:T(8,128)(2,1)S(1)}, u32[]{:S(2)}, u32[]{:S(2)}) async-start(bf16[1,8,96,512]{3,2,0,1:T(8,128)(2,1)} %bitcast.19), calls=%async_computation.3 | async-start | bytes 1572864 | tf_op jit(solution)/shard_map/all_to_all | solution.py:36
  235.0 0.1 reshape.289
  235.1 0.0 copy-done.1
  235.1 0.1 copy.73
  235.3 20.6 %all-to-all-done.3 = bf16[1,8,96,512]{3,2,0,1:T(8,128)(2,1)S(1)} async-done(((bf16[1,8,96,512]{3,2,0,1:T(8,128)(2,1)}), bf16[1,8,96,512]{3,2,0,1:T(8,128)(2,1)S(1)}, u32[]{:S(2)}, u32[]{:S(2)}) %all-to-all-start.3) | async-done | bytes 786464 | tf_op jit(solution)/shard_map/all_to_all | solution.py:36
  255.9 0.1 pad_maximum_fusion
  256.1 0.1 copy.71
  256.2 4.0 %gather_fusion = bf16[1024,512]{1,0:T(8,128)(2,1)S(1)} fusion(bf16[1536,512]{1,0:T(8,128)(2,1)S(1)} %bitcast.78, s32[1024]{0:T(1024)S(1)} %broadcast_clamp_fusion), kind=kCustom, calls=%fused_computation | custom fusion | bytes 2101248 | tf_op jit(solution)/shard_map/gather | solution.py:86
  260.2 0.7 reshape.290
  260.9 2.1 multiply_reduce_fusion
  (8 shorter events, 0.1 us)
Async XLA Ops:
  6.5 8.8 %copy-start = (bf16[256,2048]{1,0:T(8,128)(2,1)S(1)}, bf16[256,2048]{1,0:T(8,128)(2,1)}, u32[]{:S(2)}) copy-start(bf16[256,2048]{1,0:T(8,128)(2,1)} %param.7) | copy-start | bytes 3145732
  6.5 82.1 %all-gather.7.cloned.1.call-start = ((), (), s32[]{:S(2)}) async-start(), calls=%async_computation.4 | async-start | bytes 3932160 | tf_op jit(solution)/shard_map/all_gather | solution.py:22
  45.8 88.4 %all-gather.9.cloned.1.call-start = ((), (), s32[]{:S(2)}) async-start(), calls=%async_computation.5 | async-start | bytes 3932160 | tf_op jit(solution)/shard_map/all_gather | solution.py:22
  69.9 109.8 %all-gather.11.cloned.1.call-start = ((), (), s32[]{:S(2)}) async-start(), calls=%async_computation.6 | async-start | bytes 3932160 | tf_op jit(solution)/shard_map/all_gather | solution.py:31
  88.6 4.5 %copy-start.2 = (bf16[2,2048,512]{2,1,0:T(8,128)(2,1)S(1)}, bf16[2,2048,512]{2,1,0:T(8,128)(2,1)}, u32[]{:S(2)}) copy-start(bf16[2,2048,512]{2,1,0:T(8,128)(2,1)} %param.12) | copy-start | bytes 12582916
  88.6 4.7 %copy-start.5 = (bf16[1,768,2048]{2,1,0:T(8,128)(2,1)S(1)}, bf16[1,768,2048]{2,1,0:T(8,128)(2,1)}, u32[]{:S(2)}) copy-start(bf16[1,768,2048]{2,1,0:T(8,128)(2,1)} %all-gather.7.cloned.1.call-done) | copy-start | bytes 9437188
  96.4 128.8 %all-gather.13.cloned.1.call-start = ((), (), s32[]{:S(2)}) async-start(), calls=%async_computation.7 | async-start | bytes 3932160 | tf_op jit(solution)/shard_map/all_gather | solution.py:31
  134.2 4.5 %copy-start.3 = (bf16[2,2048,512]{2,1,0:T(8,128)(2,1)S(1)}, bf16[2,2048,512]{2,1,0:T(8,128)(2,1)}, u32[]{:S(2)}) copy-start(bf16[2,2048,512]{2,1,0:T(8,128)(2,1)} %param.12) | copy-start | bytes 12582916
  134.2 4.7 %copy-start.4 = (bf16[1,768,2048]{2,1,0:T(8,128)(2,1)S(1)}, bf16[1,768,2048]{2,1,0:T(8,128)(2,1)}, u32[]{:S(2)}) copy-start(bf16[1,768,2048]{2,1,0:T(8,128)(2,1)} %all-gather.9.cloned.1.call-done) | copy-start | bytes 9437188
  185.0 45.4 %all-to-all-start.1 = ((bf16[1,8,96,512]{3,2,0,1:T(8,128)(2,1)}), bf16[1,8,96,512]{3,2,0,1:T(8,128)(2,1)S(1)}, u32[]{:S(2)}, u32[]{:S(2)}) async-start(bf16[1,8,96,512]{3,2,0,1:T(8,128)(2,1)} %bitcast.10), calls=%async_computation.1 | async-start | bytes 1572864 | tf_op jit(solution)/shard_map/all_to_all | solution.py:36
  189.6 45.5 %copy-start.1 = (f32[256,4]{0,1:T(4,128)S(1)}, f32[256,4]{0,1:T(4,128)}, u32[]{:S(2)}) copy-start(f32[256,4]{0,1:T(4,128)} %param.10) | copy-start | bytes 12292
  230.4 25.6 %all-to-all-start.3 = ((bf16[1,8,96,512]{3,2,0,1:T(8,128)(2,1)}), bf16[1,8,96,512]{3,2,0,1:T(8,128)(2,1)S(1)}, u32[]{:S(2)}, u32[]{:S(2)}) async-start(bf16[1,8,96,512]{3,2,0,1:T(8,128)(2,1)} %bitcast.19), calls=%async_computation.3 | async-start | bytes 1572864 | tf_op jit(solution)/shard_map/all_to_all | solution.py:36
Sparse Core Ops, SparseCore 0:
  45.9 42.6 all-gather.6
  90.4 43.6 all-gather.8
  136.0 43.6 all-gather.10
  181.4 43.6 all-gather.12
where the time goes:
time: 270 us; the launch traced here: 269 us
  waiting for transfers between devices  150 us (56%)
  blocking collectives  51.2 us (19%)
  matrix products  27 us (10%)
  between operations  13.3 us (5%)
  other arithmetic  10 us (4%)
  starting transfers between devices  9.36 us (3%)
  local copies, waits for them, and re-layouts  8.03 us (3%)
    all_gather x2, waiting for transfers between devices, expert_work(): lax.all_gather(activation, 'tp', axis=2, tiled=True)  73.4 us
    all_gather x2, waiting for transfers between devices, expert_work(): shard_piece = lax.all_gather(row_block, 'tp', axis=2, tiled=True)  56.4 us
    all_to_all x2, blocking collectives, expert_work(): lax.all_to_all(outgoing, 'ep', split_axis=1, concat_axis=1, tiled=True)  51.2 us
    all_to_all x2, waiting for transfers between devices, expert_work(): return lax.all_to_all(result, 'ep', split_axis=1, concat_axis=1, tiled=True)  20.6 us
    dot_general x2, matrix products, expert_work(): jnp.einsum('lrf,lfd->lrd', lax.all_gather(activation, 'tp', axis=2, tiled...  10.4 us
    all_to_all x2, starting transfers between devices, expert_work(): return lax.all_to_all(result, 'ep', split_axis=1, concat_axis=1, tiled=True)  9.23 us
    dot_general x2, matrix products, expert_work(): jnp.einsum('lrd,ldf->lrf', shard_piece, gate_weight, preferred_element_ty...  8.95 us
    dot_general x2, matrix products, expert_work(): jnp.einsum('lrd,ldf->lrf', shard_piece, up_weight, preferred_element_type...  5.99 us
  transfers between devices with their start and end apart: 6, of which 5 were waited for; matrix products, arithmetic and copies ran while one was open for 10% of the time, Pallas kernels for 0%

commit v1 on v0

--- a/solution.py
+++ b/solution.py
@@ -15,6 +15,20 @@
 
 
 def expert_work(outgoing, gate_weight, up_weight, down_weight):
+
+    def lines_remake(content, lane_axis, out_dim, u_in):
+        z_new = jax.lax.axis_size(lane_axis)
+        e_next, odd = (z_new, jax.lax.axis_index(lane_axis))
+        n_now = content.shape[out_dim]
+        store = [(b, (b - 1) % e_next) for b in range(e_next)]
+        block_now = content
+        r2 = u_in(block_now, odd * n_now)
+        for u in range(1, e_next):
+            block_now = jax.lax.ppermute(block_now, lane_axis, store)
+            mid_arr = u_in(block_now, (odd + u) % e_next * n_now)
+            r2 = r2 + mid_arr
+        return r2
+
     received = lax.all_to_all(outgoing, "ep", split_axis=1, concat_axis=1, tiled=True)
     local_count, sources, capacity, columns = received.shape
     row_count = sources * capacity
@@ -26,11 +40,16 @@
     up_sum = jnp.einsum("lrd,ldf->lrf", shard_piece, up_weight, preferred_element_type=jnp.float32)
     activation = clamped_units(gate_sum, up_sum).astype(jnp.bfloat16)
     out_cols = down_weight.shape[2]
-    result = jnp.einsum(
-        "lrf,lfd->lrd",
-        lax.all_gather(activation, "tp", axis=2, tiled=True),
-        down_weight,
-        preferred_element_type=jnp.float32,
+    result = lines_remake(
+        activation,
+        "tp",
+        out_dim=2,
+        u_in=lambda own_block, start: jnp.einsum(
+            "lrf,lfd->lrd",
+            own_block,
+            lax.dynamic_slice_in_dim(down_weight, start, own_block.shape[2], axis=1),
+            preferred_element_type=jnp.float32,
+        ),
     )
     result = result.astype(jnp.bfloat16).reshape(local_count, sources, capacity, out_cols)
     return lax.all_to_all(result, "ep", split_axis=1, concat_axis=1, tiled=True)

time: 270 us -> 284 us (1.052)
  starting transfers between devices: 9.36 us -> 21 us
  waiting for transfers between devices: 150 us -> 154 us
    all_gather x2 -> x0, waiting for transfers between devices: 73.4 us -> none  [expert_work(): lax.all_gather(activation, 'tp', axis=2, tiled=True)]
    ppermute x0 -> x6, waiting for transfers between devices: none -> 63.4 us  [lines_remake(): block_now = jax.lax.ppermute(block_now, lane_axis, store)]
    all_gather x2, waiting for transfers between devices: 56.4 us -> 70.4 us  [expert_work(): shard_piece = lax.all_gather(row_block, 'tp', axis=2, tiled=True)]
    ppermute x0 -> x6, starting transfers between devices: none -> 11.6 us  [lines_remake(): block_now = jax.lax.ppermute(block_now, lane_axis, store)]
    dot_general x2 -> x8, matrix products: 10.4 us -> 9.75 us  [expert_work(): jnp.einsum('lrf,lfd->lrd', own_block, lax.dynamic_slice_in_dim(down_weigh...]
  transfers between devices with their start and end apart: 6 -> 10, of which waited for: 5 -> 8; matrix products, arithmetic and copies ran while one was open for 10% -> 8% of each run, Pallas kernels for 0% -> 0%
where the time goes in v1:
time: 284 us; the launch traced here: 283 us
  waiting for transfers between devices  154 us (54%)
  blocking collectives  51.3 us (18%)
  matrix products  24.6 us (9%)
  starting transfers between devices  21 us (7%)
  between operations  13.6 us (5%)
  other arithmetic  10 us (4%)
  local copies, waits for them, and re-layouts  8.09 us (3%)
    all_gather x2, waiting for transfers between devices, expert_work(): shard_piece = lax.all_gather(row_block, 'tp', axis=2, tiled=True)  70.4 us
    ppermute x6, waiting for transfers between devices, lines_remake(): block_now = jax.lax.ppermute(block_now, lane_axis, store)  63.4 us
    all_to_all x2, blocking collectives, expert_work(): lax.all_to_all(outgoing, 'ep', split_axis=1, concat_axis=1, tiled=True)  51.3 us
    all_to_all x2, waiting for transfers between devices, expert_work(): return lax.all_to_all(result, 'ep', split_axis=1, concat_axis=1, tiled=True)  20.6 us
    ppermute x6, starting transfers between devices, lines_remake(): block_now = jax.lax.ppermute(block_now, lane_axis, store)  11.6 us
    dot_general x8, matrix products, expert_work(): jnp.einsum('lrf,lfd->lrd', own_block, lax.dynamic_slice_in_dim(down_weigh...  9.75 us
    all_to_all x2, starting transfers between devices, expert_work(): return lax.all_to_all(result, 'ep', split_axis=1, concat_axis=1, tiled=True)  9.35 us
    dot_general x2, matrix products, expert_work(): jnp.einsum('lrd,ldf->lrf', shard_piece, gate_weight, preferred_element_ty...  8.93 us
  transfers between devices with their start and end apart: 10, of which 8 were waited for; matrix products, arithmetic and copies ran while one was open for 8% of the time, Pallas kernels for 0%

profile of v1, /device:TPU:0, one launch (start us, length us, event | category | flops | bytes accessed | tf_op | source)
XLA Modules:
  0.0 283.1 jit_solution(9522714354775366519)
XLA Ops:
  6.5 0.9 copy.62
  7.4 0.1 eq.51
  7.6 0.1 eq.47
  7.7 4.5 %reduce-window.6 = s32[16,8,128]{2,1,0:T(8,128)S(1)} reduce-window(s32[16,8,128]{2,1,0:T(8,128)S(1)} %fusion.58, s32[]{:T(128)} %constant.75.clone.1), window={size=1x1x128 pad=0_0x0_0x127_0}, to_apply=%region_0.0 | reduce-window | flops 2080768 | bytes 131076 | tf_op jit(solution)/shard_map/reduce-window
  12.2 0.1 slice.50
  12.3 0.1 copy.64
  12.5 0.1 copy.65
  12.5 0.1 broadcast_add_fusion
  12.7 0.1 reduce_sum.41
  12.8 0.1 copy.66
  12.9 0.7 fusion.61
  13.6 1.7 fusion
  15.3 0.2 convert_reduce_fusion
  15.6 0.4 multiply_reduce_fusion.1
  16.0 0.8 dynamic_slice.31
  16.8 1.7 convolution_convert_fusion
  18.5 0.1 fusion.78
  18.6 27.2 %all_to_all.20 = bf16[1,8,96,512]{3,2,0,1:T(8,128)(2,1)} all-to-all(bf16[1,8,96,512]{3,2,0,1:T(8,128)(2,1)S(1)} %bitcast.116), channel_id=1, replica_groups=mesh['ep'=8,'tp'=4] {'ep'}, dimensions={1} | all-to-all | bytes 1572864 | tf_op jit(solution)/shard_map/all_to_all | solution.py:32
  45.8 0.0 all-gather.3.cloned.1.call-update
  45.8 0.0 all-gather.5.cloned.1.call-start
  45.8 24.1 %all_to_all.21 = bf16[1,8,96,512]{3,2,0,1:T(8,128)(2,1)} all-to-all(bf16[1,8,96,512]{3,2,0,1:T(8,128)(2,1)S(1)} %bitcast.115), channel_id=1, replica_groups=mesh['ep'=8,'tp'=4] {'ep'}, dimensions={1} | all-to-all | bytes 1572864 | tf_op jit(solution)/shard_map/all_to_all | solution.py:32
  69.9 0.0 all-gather.5.cloned.1.call-update
  69.9 18.7 %all-gather.3.cloned.1.call-done = bf16[1,768,2048]{2,1,0:T(8,128)(2,1)} async-done(((bf16[1,768,512]{2,1,0:T(8,128)(2,1)}), bf16[1,768,2048]{2,1,0:T(8,128)(2,1)}) %all-gather.3.cloned.1.call-update) | async-done | bytes 3145744 | tf_op jit(solution)/shard_map/all_gather | solution.py:36
  88.6 4.5 %fusion.7 = f32[768,512]{1,0:T(8,128)S(1)} fusion(bf16[1,768,2048]{2,1,0:T(8,128)(2,1)} %all-gather.3.cloned.1.call-done, bf16[2,2048,512]{2,1,0:T(8,128)(2,1)} %param.11), kind=kOutput, calls=%fused_computation.9 | convolution fusion | flops 1610612736 | bytes 6815744 | tf_op jit(solution)/shard_map/lrd,ldf->lrf/dot_general | solution.py:37
  93.1 0.3 copy-done.9
  93.3 2.1 multiply_convert_fusion.1
  95.5 1.5 collective-permute-start
  97.0 51.7 %all-gather.5.cloned.1.call-done = bf16[1,768,2048]{2,1,0:T(8,128)(2,1)} async-done(((bf16[1,768,512]{2,1,0:T(8,128)(2,1)}), bf16[1,768,2048]{2,1,0:T(8,128)(2,1)}) %all-gather.5.cloned.1.call-update) | async-done | bytes 3145744 | tf_op jit(solution)/shard_map/all_gather | solution.py:36
  148.7 4.5 %fusion.3 = f32[768,512]{1,0:T(8,128)S(1)} fusion(bf16[1,768,2048]{2,1,0:T(8,128)(2,1)} %all-gather.5.cloned.1.call-done, bf16[2,2048,512]{2,1,0:T(8,128)(2,1)} %param.11), kind=kOutput, calls=%fused_computation.5 | convolution fusion | flops 1610612736 | bytes 6815744 | tf_op jit(solution)/shard_map/lrd,ldf->lrf/dot_general | solution.py:37
  153.2 0.0 copy-done.2
  153.2 0.0 collective-permute-done
  153.2 1.5 collective-permute-start.1
  154.7 2.1 multiply_convert_fusion
  156.8 0.0 copy-start.4
  156.8 0.0 copy-start.3
  156.8 1.5 collective-permute-start.3
  158.4 0.3 fusion.77
  158.7 15.0 %collective-permute-done.1 = bf16[1,768,512]{2,1,0:T(8,128)(2,1)S(1)} collective-permute-done((bf16[1,768,512]{2,1,0:T(8,128)(2,1)S(1)}, bf16[1,768,512]{2,1,0:T(8,128)(2,1)S(1)}, u32[]{:S(2)}, u32[]{:S(2)}) %collective-permute-start.1) | collective-permute-done | bytes 786464 | tf_op jit(solution)/shard_map/ppermute | solution.py:27
  173.7 2.4 collective-permute-start.2
  176.0 0.6 fusion.43
  176.6 14.0 %collective-permute-done.3 = bf16[1,768,512]{2,1,0:T(8,128)(2,1)} collective-permute-done((bf16[1,768,512]{2,1,0:T(8,128)(2,1)S(1)}, bf16[1,768,512]{2,1,0:T(8,128)(2,1)}, u32[]{:S(2)}, u32[]{:S(2)}) %collective-permute-start.3) | collective-permute-done | bytes 786464 | tf_op jit(solution)/shard_map/ppermute | solution.py:27
  190.6 2.4 collective-permute-start.4
  193.0 0.6 fusion.33
  193.5 0.6 fusion.31
  194.1 13.2 %collective-permute-done.2 = bf16[1,768,512]{2,1,0:T(8,128)(2,1)S(1)} collective-permute-done((bf16[1,768,512]{2,1,0:T(8,128)(2,1)S(1)}, bf16[1,768,512]{2,1,0:T(8,128)(2,1)S(1)}, u32[]{:S(2)}, u32[]{:S(2)}) %collective-permute-start.2) | collective-permute-done | bytes 786464 | tf_op jit(solution)/shard_map/ppermute | solution.py:27
  207.4 1.5 add_convert_fusion.1
  208.8 4.6 %all-to-all-start.1 = ((bf16[1,8,96,512]{3,2,0,1:T(8,128)(2,1)}), bf16[1,8,96,512]{3,2,0,1:T(8,128)(2,1)S(1)}, u32[]{:S(2)}, u32[]{:S(2)}) async-start(bf16[1,8,96,512]{3,2,0,1:T(8,128)(2,1)} %bitcast.117), calls=%async_computation.1 | async-start | bytes 1572864 | tf_op jit(solution)/shard_map/all_to_all | solution.py:55
  213.4 9.6 %collective-permute-done.4 = bf16[1,768,512]{2,1,0:T(8,128)(2,1)} collective-permute-done((bf16[1,768,512]{2,1,0:T(8,128)(2,1)}, bf16[1,768,512]{2,1,0:T(8,128)(2,1)}, u32[]{:S(2)}, u32[]{:S(2)}) %collective-permute-start.4) | collective-permute-done | bytes 786464 | tf_op jit(solution)/shard_map/ppermute | solution.py:27
  223.0 2.4 collective-permute-start.5
  225.4 1.7 fusion.38
  227.1 1.7 fusion.28
  228.8 1.7 fusion.26
  230.5 11.6 %collective-permute-done.5 = bf16[1,768,512]{2,1,0:T(8,128)(2,1)S(1)} collective-permute-done((bf16[1,768,512]{2,1,0:T(8,128)(2,1)}, bf16[1,768,512]{2,1,0:T(8,128)(2,1)S(1)}, u32[]{:S(2)}, u32[]{:S(2)}) %collective-permute-start.5) | collective-permute-done | bytes 786464 | tf_op jit(solution)/shard_map/ppermute | solution.py:27
  242.1 1.5 add_convert_fusion
  243.6 0.0 all-to-all-done.1
  243.6 4.7 %all-to-all-start.3 = ((bf16[1,8,96,512]{3,2,0,1:T(8,128)(2,1)}), bf16[1,8,96,512]{3,2,0,1:T(8,128)(2,1)S(1)}, u32[]{:S(2)}, u32[]{:S(2)}) async-start(bf16[1,8,96,512]{3,2,0,1:T(8,128)(2,1)} %bitcast.118), calls=%async_computation.3 | async-start | bytes 1572864 | tf_op jit(solution)/shard_map/all_to_all | solution.py:55
  248.3 0.1 reshape.345
  248.5 0.1 copy.73
  248.7 20.6 %all-to-all-done.3 = bf16[1,8,96,512]{3,2,0,1:T(8,128)(2,1)S(1)} async-done(((bf16[1,8,96,512]{3,2,0,1:T(8,128)(2,1)}), bf16[1,8,96,512]{3,2,0,1:T(8,128)(2,1)S(1)}, u32[]{:S(2)}, u32[]{:S(2)}) %all-to-all-start.3) | async-done | bytes 786464 | tf_op jit(solution)/shard_map/all_to_all | solution.py:55
  269.3 0.1 pad_maximum_fusion
  269.4 0.1 copy.71
  269.5 4.0 %gather_fusion = bf16[1024,512]{1,0:T(8,128)(2,1)S(1)} fusion(bf16[1536,512]{1,0:T(8,128)(2,1)S(1)} %bitcast.112, s32[1024]{0:T(1024)S(1)} %broadcast_clamp_fusion), kind=kCustom, calls=%fused_computation | custom fusion | bytes 2101248 | tf_op jit(solution)/shard_map/gather | solution.py:105
  273.5 0.7 reshape.346
  274.2 2.1 multiply_reduce_fusion
  (25 shorter events, 0.2 us)
Async XLA Ops:
  6.5 8.8 %copy-start.1 = (bf16[256,2048]{1,0:T(8,128)(2,1)S(1)}, bf16[256,2048]{1,0:T(8,128)(2,1)}, u32[]{:S(2)}) copy-start(bf16[256,2048]{1,0:T(8,128)(2,1)} %param.7) | copy-start | bytes 3145732
  6.5 82.1 %all-gather.3.cloned.1.call-start = ((), (), s32[]{:S(2)}) async-start(), calls=%async_computation.4 | async-start | bytes 3932160 | tf_op jit(solution)/shard_map/all_gather | solution.py:36
  45.8 102.9 %all-gather.5.cloned.1.call-start = ((), (), s32[]{:S(2)}) async-start(), calls=%async_computation.5 | async-start | bytes 3932160 | tf_op jit(solution)/shard_map/all_gather | solution.py:36
  88.6 4.5 %copy-start.6 = (bf16[2,2048,512]{2,1,0:T(8,128)(2,1)S(1)}, bf16[2,2048,512]{2,1,0:T(8,128)(2,1)}, u32[]{:S(2)}) copy-start(bf16[2,2048,512]{2,1,0:T(8,128)(2,1)} %param.12) | copy-start | bytes 12582916
  88.6 4.7 %copy-start.9 = (bf16[1,768,2048]{2,1,0:T(8,128)(2,1)S(1)}, bf16[1,768,2048]{2,1,0:T(8,128)(2,1)}, u32[]{:S(2)}) copy-start(bf16[1,768,2048]{2,1,0:T(8,128)(2,1)} %all-gather.3.cloned.1.call-done) | copy-start | bytes 9437188
  95.4 57.7 %copy-start.2 = (bf16[768,512]{1,0:T(8,128)(2,1)}, bf16[768,512]{1,0:T(8,128)(2,1)S(1)}, u32[]{:S(2)}) copy-start(bf16[768,512]{1,0:T(8,128)(2,1)S(1)} %multiply_convert_fusion.1) | copy-start | bytes 2359300
  95.5 57.7 %collective-permute-start = (bf16[1,768,512]{2,1,0:T(8,128)(2,1)S(1)}, bf16[1,768,512]{2,1,0:T(8,128)(2,1)S(1)}, u32[]{:S(2)}, u32[]{:S(2)}) collective-permute-start(bf16[1,768,512]{2,1,0:T(8,128)(2,1)S(1)} %bitcast.119), channel_id=1, source_target_pairs={{0,3},{1,0},{2,1},{3,2},{4,7},{5,4},{6,5},{7,6},{8,11},{9,8},{10,9... | collective-permute-start | bytes 2359304 | tf_op jit(solution)/shard_map/ppermute | solution.py:27
  148.7 6.0 %copy-start.7 = (bf16[2,2048,512]{2,1,0:T(8,128)(2,1)S(1)}, bf16[2,2048,512]{2,1,0:T(8,128)(2,1)}, u32[]{:S(2)}) copy-start(bf16[2,2048,512]{2,1,0:T(8,128)(2,1)} %param.12) | copy-start | bytes 12582916
  148.7 6.0 %copy-start.8 = (bf16[1,768,2048]{2,1,0:T(8,128)(2,1)S(1)}, bf16[1,768,2048]{2,1,0:T(8,128)(2,1)}, u32[]{:S(2)}) copy-start(bf16[1,768,2048]{2,1,0:T(8,128)(2,1)} %all-gather.5.cloned.1.call-done) | copy-start | bytes 9437188
  153.2 20.5 %collective-permute-start.1 = (bf16[1,768,512]{2,1,0:T(8,128)(2,1)S(1)}, bf16[1,768,512]{2,1,0:T(8,128)(2,1)S(1)}, u32[]{:S(2)}, u32[]{:S(2)}) collective-permute-start(bf16[1,768,512]{2,1,0:T(8,128)(2,1)S(1)} %collective-permute-done), channel_id=1, source_target_pairs={{0,3},{1,0},{2,1},{3,2},{4,7},{5,4},{6,5},{7,6},{8,11},{9,8},{10,9... | collective-permute-start | bytes 2359304 | tf_op jit(solution)/shard_map/ppermute | solution.py:27
  154.7 3.7 %copy-start = (bf16[2,2048,512]{2,1,0:T(8,128)(2,1)S(1)}, bf16[2,2048,512]{2,1,0:T(8,128)(2,1)}, u32[]{:S(2)}) copy-start(bf16[2,2048,512]{2,1,0:T(8,128)(2,1)} %param.13) | copy-start | bytes 12582916
  156.8 1.8 copy-start.4
  156.8 19.2 %copy-start.3 = (bf16[768,512]{1,0:T(8,128)(2,1)S(1)}, bf16[768,512]{1,0:T(8,128)(2,1)}, u32[]{:S(2)}) copy-start(bf16[768,512]{1,0:T(8,128)(2,1)} %copy-done.2) | copy-start | bytes 2359300
  156.8 33.8 %collective-permute-start.3 = (bf16[1,768,512]{2,1,0:T(8,128)(2,1)S(1)}, bf16[1,768,512]{2,1,0:T(8,128)(2,1)}, u32[]{:S(2)}, u32[]{:S(2)}) collective-permute-start(bf16[1,768,512]{2,1,0:T(8,128)(2,1)S(1)} %bitcast.120), channel_id=1, source_target_pairs={{0,3},{1,0},{2,1},{3,2},{4,7},{5,4},{6,5},{7,6},{8,11},{9,8},{10,9... | collective-permute-start | bytes 2359304 | tf_op jit(solution)/shard_map/ppermute | solution.py:27
  173.7 33.7 %collective-permute-start.2 = (bf16[1,768,512]{2,1,0:T(8,128)(2,1)S(1)}, bf16[1,768,512]{2,1,0:T(8,128)(2,1)S(1)}, u32[]{:S(2)}, u32[]{:S(2)}) collective-permute-start(bf16[1,768,512]{2,1,0:T(8,128)(2,1)S(1)} %collective-permute-done.1), channel_id=1, source_target_pairs={{0,3},{1,0},{2,1},{3,2},{4,7},{5,4},{6,5},{7,6},{8,11},{9,8},{10,9... | collective-permute-start | bytes 2359304 | tf_op jit(solution)/shard_map/ppermute | solution.py:27
  190.6 32.4 %collective-permute-start.4 = (bf16[1,768,512]{2,1,0:T(8,128)(2,1)}, bf16[1,768,512]{2,1,0:T(8,128)(2,1)}, u32[]{:S(2)}, u32[]{:S(2)}) collective-permute-start(bf16[1,768,512]{2,1,0:T(8,128)(2,1)} %collective-permute-done.3), channel_id=1, source_target_pairs={{0,3},{1,0},{2,1},{3,2},{4,7},{5,4},{6,5},{7,6},{8,11},{9,8},{10,9... | collective-permute-start | bytes 2359304 | tf_op jit(solution)/shard_map/ppermute | solution.py:27
  208.8 34.8 %all-to-all-start.1 = ((bf16[1,8,96,512]{3,2,0,1:T(8,128)(2,1)}), bf16[1,8,96,512]{3,2,0,1:T(8,128)(2,1)S(1)}, u32[]{:S(2)}, u32[]{:S(2)}) async-start(bf16[1,8,96,512]{3,2,0,1:T(8,128)(2,1)} %bitcast.117), calls=%async_computation.1 | async-start | bytes 1572864 | tf_op jit(solution)/shard_map/all_to_all | solution.py:55
  223.0 19.1 %collective-permute-start.5 = (bf16[1,768,512]{2,1,0:T(8,128)(2,1)}, bf16[1,768,512]{2,1,0:T(8,128)(2,1)S(1)}, u32[]{:S(2)}, u32[]{:S(2)}) collective-permute-start(bf16[1,768,512]{2,1,0:T(8,128)(2,1)} %collective-permute-done.4), channel_id=1, source_target_pairs={{0,3},{1,0},{2,1},{3,2},{4,7},{5,4},{6,5},{7,6},{8,11},{9,8},{10,9... | collective-permute-start | bytes 2359304 | tf_op jit(solution)/shard_map/ppermute | solution.py:27
  243.6 4.9 %copy-start.5 = (f32[256,4]{0,1:T(4,128)S(1)}, f32[256,4]{0,1:T(4,128)}, u32[]{:S(2)}) copy-start(f32[256,4]{0,1:T(4,128)} %param.10) | copy-start | bytes 12292
  243.6 25.7 %all-to-all-start.3 = ((bf16[1,8,96,512]{3,2,0,1:T(8,128)(2,1)}), bf16[1,8,96,512]{3,2,0,1:T(8,128)(2,1)S(1)}, u32[]{:S(2)}, u32[]{:S(2)}) async-start(bf16[1,8,96,512]{3,2,0,1:T(8,128)(2,1)} %bitcast.118), calls=%async_computation.3 | async-start | bytes 1572864 | tf_op jit(solution)/shard_map/all_to_all | solution.py:55
Sparse Core Ops, SparseCore 0:
  45.9 42.6 all-gather.2
  90.4 58.2 all-gather.4
